TPU v7x, 128 devices: a 2x2x16 block of a 8x8x16 slice. The times are simulated.
128 devices in a mesh: grp: 4 (over y, x), ep: 32 (over z, core).
Axes of the slice: x: 2, y: 2, z: 16, core: 2. Of those that a mesh axis runs over, the one named last changes fastest.
The devices are a block of a 8x8x16 slice.
Arguments:
- tokens: bfloat16 [4096, 2048], P(('grp', 'ep')), parts along dimension 0, may hold values from -6 to 6
- routes: int32 [4096, 8], P(('grp', 'ep')), parts along dimension 0, may hold values from 0 to 31, all different within a row; in each aligned block of 32 rows (0 to 31, 32 to 63, ...) at most 24 rows name the same one
- gates: float32 [4096, 8], P(('grp', 'ep')), parts along dimension 0, may hold values from 0.1 to 0.6
- norm_gain: float32 [2048], replicated, may hold values from 0.1 to 1.9
- expert_gate: bfloat16 [32, 2048, 512], P('ep'), may hold values from -0.125 to 0.125
- expert_up: bfloat16 [32, 2048, 512], P('ep'), may hold values from -0.125 to 0.125
- expert_down: bfloat16 [32, 512, 2048], P('ep'), may hold values from -0.25 to 0.25
- shared_gate: bfloat16 [2048, 512], replicated, may hold values from -0.125 to 0.125
- shared_up: bfloat16 [2048, 512], replicated, may hold values from -0.125 to 0.125
- shared_down: bfloat16 [512, 2048], replicated, may hold values from -0.25 to 0.25
Outputs:
- mixed: bfloat16 [4096, 2048], P(('grp', 'ep')), parts along dimension 0
There are 4 independent parts, one for each index of `grp`. A program takes and returns all parts, laid end to end along the dimension named above; an argument that names none is the same for every part. Nothing has to cross between parts.
Inputs may be any that keep to these rules, and one draw needn't show every extreme that they name: `routes`: each row names 8 different experts; among the rows of one device no expert is named by more than 24 rows, a bound that some block reaches.
All inputs are finite; a program needn't handle non-finite values.
Results may differ from a plain program's by a relative error of at most 0.013.
Values may be sent and summed in bfloat16 or wider, within the bound.
A program may use at most 128 MiB of HBM per device.

v0:
```python
import jax
import jax.numpy as jnp
from jax import lax
from jax.sharding import Mesh
from jax.sharding import PartitionSpec as P

EP = ("ep_0", "ep_1")
GRP_EP = ("grp", "ep_0", "ep_1")


def summed_rows(x, axes, dim):
    for axis in axes:
        x = lax.psum_scatter(x, axis, scatter_dimension=dim, tiled=True)
    return x


def norm_rows(tokens, norm_gain):
    values = tokens.astype(jnp.float32)
    scale = lax.rsqrt(jnp.mean(values * values, axis=-1, keepdims=True) + 1e-06)
    return (values * scale * norm_gain).astype(jnp.bfloat16)


def expert_rows(in_rows, w_gate, w_up, w_down):
    gate_pre = jnp.dot(in_rows, w_gate, preferred_element_type=jnp.float32)
    up_pre = jnp.dot(in_rows, w_up, preferred_element_type=jnp.float32)
    hidden = (jax.nn.silu(gate_pre) * up_pre).astype(jnp.bfloat16)
    return jnp.dot(hidden, w_down, preferred_element_type=jnp.float32).astype(jnp.bfloat16)


def slot_table(marks, capacity):
    before = jnp.cumsum(marks, axis=1) - marks
    slot_ids = jnp.arange(capacity, dtype=jnp.int32)
    picked = marks[:, None, :] * (before[:, None, :] == slot_ids[None, :, None]).astype(jnp.int32)
    places = jnp.arange(marks.shape[1], dtype=jnp.int32)
    return (jnp.sum(picked * places[None, None, :], axis=2), jnp.sum(picked, axis=2), before)


def shared_terms(normed, shared_gate, shared_up, shared_down):
    gate_pre = jnp.dot(normed, shared_gate, preferred_element_type=jnp.float32)
    up_pre = jnp.dot(normed, shared_up, preferred_element_type=jnp.float32)
    shared_hidden = (jax.nn.silu(gate_pre) * up_pre).astype(jnp.bfloat16)
    return jnp.dot(shared_hidden, shared_down, preferred_element_type=jnp.float32)


def local(
    tokens,
    routes,
    gates,
    norm_gain,
    expert_gate,
    expert_up,
    expert_down,
    shared_gate,
    shared_up,
    shared_down,
):
    rows_dev = tokens.shape[0]
    width = tokens.shape[1]
    groups = lax.axis_size(EP)
    capacity = 3 * rows_dev // 4
    normed = norm_rows(tokens, norm_gain)
    w_gate = expert_gate[0]
    w_up = expert_up[0]
    w_down = expert_down[0]
    shared = shared_terms(normed, shared_gate, shared_up, shared_down)
    gathered, all_routes, all_gates = (
        lax.all_gather(normed, EP, axis=0, tiled=True),
        lax.all_gather(routes, EP, axis=0, tiled=True),
        lax.all_gather(gates.astype(jnp.bfloat16), EP, axis=0, tiled=True).astype(gates.dtype),
    )
    own_expert = lax.axis_index(EP)
    matched = all_routes == own_expert
    marks = jnp.sum(matched.astype(jnp.int32), axis=1).reshape(groups, rows_dev)
    slot_rows, filled, before = slot_table(marks, capacity)
    source = (slot_rows + jnp.arange(groups, dtype=jnp.int32)[:, None] * rows_dev).reshape(-1)
    answers = expert_rows(jnp.take(gathered, source, axis=0), w_gate, w_up, w_down)
    token_weight = jnp.sum(jnp.where(matched, all_gates, 0.0), axis=1)
    weight = jnp.take(token_weight, source) * filled.reshape(-1).astype(jnp.float32)
    partial_value = jnp.zeros((gathered.shape[0], width), jnp.float32)
    partial_value = partial_value.at[source].add(weight[:, None] * answers.astype(jnp.float32))
    routed = summed_rows(partial_value.astype(jnp.bfloat16), EP, 0).astype(jnp.float32)
    return (routed + shared).astype(jnp.bfloat16)


def solution(mesh):
    finer = Mesh(mesh.devices.reshape(mesh.shape["grp"], 16, 2), ("grp", "ep_0", "ep_1"))
    in_specs = (
        P(GRP_EP, None),
        P(GRP_EP, None),
        P(GRP_EP, None),
        P(),
        P(EP, None, None),
        P(EP, None, None),
        P(EP, None, None),
        P(),
        P(),
        P(),
    )
    out_specs = P(GRP_EP, None)
    return jax.shard_map(local, mesh=finer, in_specs=in_specs, out_specs=out_specs, check_vma=False)
```

profile of v0, /device:TPU:70, one launch (start us, length us, event | category | flops | bytes accessed | tf_op | source)
XLA Modules:
  0.0 234.4 jit_solution(3682726006224130416)
XLA Ops:
  6.5 0.0 copy-start
  6.6 0.0 all-gather.4.cloned.1.call-start
  6.6 1.2 fusion.18
  7.7 1.7 fusion.20
  9.4 0.1 all-gather.4.cloned.1.call-update
  9.5 0.1 reduce-scatter.3.cloned.1.call-start
  9.6 0.7 convert_bitcast_fusion
  10.3 39.5 %all-gather.1 = bf16[32,32,8]{1,2,0:T(8,128)(2,1)S(1)} all-gather(bf16[1,32,8]{1,2,0:T(8,128)(2,1)S(1)} %convert_bitcast_fusion), channel_id=1, replica_groups=mesh['grp'=4,'ep_0'=16,'ep_1'=2] {'ep_0','ep_1'}, dimensions={0}, use_global_device_ids=true | all-gather | bytes 16896 | tf_op jit(solution)/shard_map/all_gather | solution.py:69
  49.7 27.9 %all-gather = s32[32,32,8]{1,2,0:T(8,128)S(1)} all-gather(s32[1,32,8]{1,2,0:T(8,128)} %bitcast.21), channel_id=1, replica_groups=mesh['grp'=4,'ep_0'=16,'ep_1'=2] {'ep_0','ep_1'}, dimensions={0}, use_global_device_ids=true | all-gather | bytes 33792 | tf_op jit(solution)/shard_map/all_gather | solution.py:68
  77.6 0.1 select_reduce_fusion.1
  77.7 0.2 reduce_window_sum.14
  77.9 1.2 select_reduce_fusion
  79.1 0.1 broadcast_add_fusion
  79.2 0.1 add.91
  79.3 0.1 add.94
  79.3 0.1 reshape.123
  79.4 0.1 convert_element_type.51
  79.6 3.2 %gather_fusion = f32[768]{0:T(1024)S(1)} fusion(f32[1024]{0:T(1024)S(1)} %reshape.123, s32[1024]{0:T(1024)S(1)} %pad_clamp_fusion), kind=kCustom, calls=%fused_computation | custom fusion | bytes 9216 | tf_op jit(solution)/shard_map/jit(_take)/gather | solution.py:78
  82.8 3.1 %all-gather.4.cloned.1.call-done = bf16[1024,2048]{1,0:T(8,128)(2,1)} async-done(((bf16[32,2048]{1,0:T(8,128)(2,1)}), bf16[1024,2048]{1,0:T(8,128)(2,1)}) %all-gather.4.cloned.1.call-update) | async-done | bytes 4194320 | tf_op jit(solution)/shard_map/all_gather | solution.py:67
  85.8 9.9 %gather_fusion.1 = bf16[768,2048]{1,0:T(8,128)(2,1)} fusion(bf16[1024,2048]{1,0:T(8,128)(2,1)} %all-gather.4.cloned.1.call-done, s32[1024]{0:T(1024)S(1)} %pad_clamp_fusion), kind=kCustom, calls=%fused_computation.1 | custom fusion | bytes 6294528 | tf_op jit(solution)/shard_map/jit(_take)/gather | solution.py:76
  95.7 5.5 %fusion.9 = f32[768,512]{1,0:T(8,128)} fusion(bf16[1,2048,512]{2,1,0:T(8,128)(2,1)} %param.14, bf16[768,2048]{1,0:T(8,128)(2,1)} %gather_fusion.1, pred[768]{0:T(1024)(128)(4,1)S(1)} %get-tuple-element.8), kind=kOutput, calls=%fused_computation.15 | convolution fusion | flops 1612185600 | bytes 6816512 | tf_op jit(solution)/shard_map/dot_general | solution.py:24
  101.2 0.0 copy-done
  101.2 8.3 %convolution_convert_fusion = bf16[768,2048]{1,0:T(8,128)(2,1)} fusion(bf16[1,512,2048]{2,1,0:T(8,128)(2,1)S(1)} %copy-done, f32[768,512]{1,0:T(8,128)} %fusion.9, bf16[1,2048,512]{2,1,0:T(8,128)(2,1)} %param.15, bf16[768,2048]{1,0:T(8,128)(2,1)} %gather_fusion.1, pred[768]{0:T(1024)(128)(4,1)S(1)} %get-tuple-element.8), kind=kOutput, calls=%fused_computation.7 | convolution fusion | flops 3226730496 | bytes 12059392 | tf_op jit(solution)/shard_map/dot_general | solution.py:27
  109.5 18.8 %scatter_custom_fusion = f32[1024,2048]{1,0:T(8,128)} fusion(s32[768]{0:T(1024)S(1)} %fusion.27, bf16[768,2048]{1,0:T(8,128)(2,1)} %convolution_convert_fusion, f32[]{:T(128)} %constant.30.clone.1, f32[768]{0:T(1024)S(1)} %get-tuple-element.7), kind=kCustom, calls=%fused_computation.3 | custom fusion | flops 4718592 | bytes 11538436 | tf_op jit(solution)/shard_map/scatter-add | solution.py:80
  128.3 6.0 %convert_element_type.57 = bf16[1024,2048]{1,0:T(8,128)(2,1)} convert(f32[1024,2048]{1,0:T(8,128)} %scatter_custom_fusion) | non-fusion elementwise | flops 2097152 | bytes 12582912 | tf_op jit(solution)/shard_map/convert_element_type | solution.py:81
  134.3 0.0 copy-start.1
  134.3 0.1 reduce-scatter.3.cloned.1.call-update
  134.4 0.1 reduce-scatter.5.cloned.1.call-start
  134.5 74.5 %reduce-scatter.3.cloned.1.call-done = bf16[64,2048]{1,0:T(8,128)(2,1)} async-done(((bf16[1024,2048]{1,0:T(8,128)(2,1)}), bf16[64,2048]{1,0:T(8,128)(2,1)}) %reduce-scatter.3.cloned.1.call-update) | async-done | bytes 262160 | tf_op jit(solution)/shard_map/reduce_scatter | solution.py:13
  209.0 0.1 reduce-scatter.5.cloned.1.call-update
  209.0 0.0 copy-done.1
  209.0 2.0 fusion.33
  211.1 13.0 %reduce-scatter.5.cloned.1.call-done = bf16[32,2048]{1,0:T(8,128)(2,1)} async-done(((bf16[64,2048]{1,0:T(8,128)(2,1)}), bf16[32,2048]{1,0:T(8,128)(2,1)}) %reduce-scatter.5.cloned.1.call-update) | async-done | bytes 131088 | tf_op jit(solution)/shard_map/reduce_scatter | solution.py:13
  224.0 3.8 %fusion.5 = bf16[32,2048]{1,0:T(8,128)(2,1)} fusion(bf16[512,2048]{1,0:T(8,128)(2,1)} %param.19, bf16[32,2048]{1,0:T(8,128)(2,1)S(1)} %copy-done.1, bf16[2048,512]{1,0:T(8,128)(2,1)} %param.18, bf16[32,2048]{1,0:T(8,128)(2,1)} %reduce-scatter.5.cloned.1.call-done, f32[32,512]{1,0:T(8,128)S(1)} %fusion.33), kind=kOutput, calls=%fused_computation.11 | convolution fusion | flops 134512640 | bytes 4653056 | tf_op jit(solution)/shard_map/dot_general | solution.py:42
  (8 shorter events, 0.1 us)
Async XLA Ops:
  6.5 94.7 %copy-start = (bf16[1,512,2048]{2,1,0:T(8,128)(2,1)S(1)}, bf16[1,512,2048]{2,1,0:T(8,128)(2,1)}, u32[]{:S(2)}) copy-start(bf16[1,512,2048]{2,1,0:T(8,128)(2,1)} %param.16) | copy-start | bytes 6291460
  6.6 79.3 %all-gather.4.cloned.1.call-start = ((), (), s32[]{:S(2)}) async-start(), calls=%async_computation.2 | async-start | bytes 4325376 | tf_op jit(solution)/shard_map/all_gather | solution.py:67
  9.5 199.5 %reduce-scatter.3.cloned.1.call-start = ((), (), s32[]{:S(2)}) async-start(), calls=%async_computation.3 | async-start | bytes 4456448 | tf_op jit(solution)/shard_map/reduce_scatter | solution.py:13
  134.3 74.7 %copy-start.1 = (bf16[32,2048]{1,0:T(8,128)(2,1)S(1)}, bf16[32,2048]{1,0:T(8,128)(2,1)}, u32[]{:S(2)}) copy-start(bf16[32,2048]{1,0:T(8,128)(2,1)} %fusion.20) | copy-start | bytes 393220
  134.4 89.6 %reduce-scatter.5.cloned.1.call-start = ((), (), s32[]{:S(2)}) async-start(), calls=%async_computation.4 | async-start | bytes 393216 | tf_op jit(solution)/shard_map/reduce_scatter | solution.py:13
Sparse Core Ops, SparseCore 0:
  9.6 76.1 all-gather.3
  134.5 74.4 reduce-scatter.2
  211.3 12.6 reduce-scatter.4
where the time goes:
time: 236 us; the launch traced here: 234 us
  waiting for transfers between devices  90.7 us (38%)
  blocking collectives  67.4 us (29%)
  other arithmetic  30 us (13%)
  matrix products  19.6 us (8%)
  local copies, waits for them, and re-layouts  13.4 us (6%)
  between operations  13.2 us (6%)
    reduce_scatter x2, waiting for transfers between devices, summed_rows(): x = lax.psum_scatter(x, axis, scatter_dimension=dim, tiled=True)  87.5 us
    all_gather x1, blocking collectives, local(): lax.all_gather(gates.astype(jnp.bfloat16), EP, axis=0, tiled=True)  39.5 us
    all_gather x1, blocking collectives, local(): lax.all_gather(routes, EP, axis=0, tiled=True)  27.9 us
    scatter-add x1, other arithmetic, local(): partial_value.at[source].add(weight[:, None] * answers.astype(jnp.float32))  18.8 us
    gather x1, local copies, waits for them, and re-layouts, local(): jnp.take(gathered, source, axis=0)  9.85 us
    dot_general x1, matrix products, expert_rows(): jnp.dot(hidden, w_down, preferred_element_type=jnp.float32)  8.28 us
    convert_element_type x1, other arithmetic, local(): partial_value.astype(jnp.bfloat16)  6.01 us
    dot_general x1, matrix products, expert_rows(): gate_pre = jnp.dot(in_rows, w_gate, preferred_element_type=jnp.float32)  5.53 us
  transfers between devices with their start and end apart: 3, of which 3 were waited for; matrix products, arithmetic and copies ran while one was open for 3% of the time, Pallas kernels for 0%

commit v1 on v0

v1 whole, which is shorter than its diff:
```python
import functools

import jax
import jax.numpy as jnp
from jax import lax
from jax.experimental import pallas as pl
from jax.experimental.pallas import tpu as pltpu
from jax.sharding import PartitionSpec as P

MESH = pl.DeviceIdType.MESH
ROW_CUTS = 2
COL_CUTS = 2
LANES = 128


def layer_kernel(
    half,
    tokens_ref,
    routes_ref,
    gates_ref,
    gain_ref,
    e_gate,
    e_up,
    e_down,
    s_gate,
    s_up,
    s_down,
    out_ref,
    blocks,
    tiles,
    w_gate,
    w_up,
    w_down,
    v_gate,
    v_up,
    v_down,
    hidden,
    kept,
    given,
    taken,
    partial,
    final,
    shared,
    weight_sem,
    ring_send,
    ring_recv,
    pair_send,
    pair_recv,
    tile_send,
    tile_recv,
    tpair_send,
    tpair_recv,
    give_send,
    give_recv,
    sum_send,
    sum_recv,
    final_recv,
):
    rows, width = tokens_ref.shape
    inner = w_down.shape[0]
    chips = 2 * half
    me = lax.axis_index("ep")
    place, core = me // 2, lax.rem(me, 2)
    step_by = 1 - 2 * core
    ahead = lax.rem(place + step_by + chips, chips)
    behind = lax.rem(place - step_by + chips, chips)
    following = {"ep": ahead * 2 + core}
    previous = {"ep": behind * 2 + core}
    partner = {"ep": place * 2 + 1 - core}
    crossing = {"ep": ahead * 2 + 1 - core}

    loads = [
        pltpu.make_async_copy(e_gate.at[0], w_gate, weight_sem.at[0]),
        pltpu.make_async_copy(e_up.at[0], w_up, weight_sem.at[1]),
        pltpu.make_async_copy(e_down.at[0], w_down, weight_sem.at[2]),
        pltpu.make_async_copy(s_gate, v_gate, weight_sem.at[3]),
        pltpu.make_async_copy(s_up, v_up, weight_sem.at[4]),
        pltpu.make_async_copy(s_down, v_down, weight_sem.at[5]),
    ]
    barrier = pltpu.get_barrier_semaphore()
    for other in (previous, partner, crossing):
        pl.semaphore_signal(barrier, inc=1, device_id=other, device_id_type=MESH)
    for load in loads:
        load.start()

    values = tokens_ref[...].astype(jnp.float32)
    scale = lax.rsqrt(jnp.mean(values * values, axis=-1, keepdims=True) + 1e-06)
    blocks[0, 0:rows, :] = (values * scale * gain_ref[...]).astype(jnp.bfloat16)

    groups = rows // 8
    experts = LANES // groups
    lane = lax.broadcasted_iota(jnp.int32, (8, LANES), 1)
    tile = jnp.zeros((8, LANES), jnp.float32)
    for group in range(groups):
        for pick in range(routes_ref.shape[1]):
            where = routes_ref[group * 8:group * 8 + 8, pick:pick + 1] + group * experts
            gate = gates_ref[group * 8:group * 8 + 8, pick:pick + 1]
            tile += jnp.where(lane == where, gate, 0.0)
    tiles[0, 0] = tile

    pl.semaphore_wait(barrier, 3)

    cut_rows, cut_cols = rows // ROW_CUTS, width // COL_CUTS
    cuts = [(r * cut_rows, c * cut_cols) for r in range(ROW_CUTS) for c in range(COL_CUTS)]
    ncuts = len(cuts)

    def area(ref, at, first, cut):
        r, c = cuts[cut]
        return ref.at[at, pl.ds(first + r, cut_rows), pl.ds(c, cut_cols)]

    def remote(src, dst, send, recv, device):
        return pltpu.make_async_remote_copy(
            src_ref=src, dst_ref=dst, send_sem=send, recv_sem=recv, device_id=device, device_id_type=MESH
        )

    def ring(s, b, q):
        return remote(
            area(blocks, s, b * rows, q), area(blocks, s + 1, b * rows, q),
            ring_send.at[s, b, q], ring_recv.at[s + 1, b, q], following,
        )

    def pair(s, b, q, first):
        return remote(
            area(blocks, s, b * rows, q), area(blocks, s, first, q),
            pair_send.at[s, b, q], pair_recv.at[s, b, q], partner,
        )

    def tile_ring(s, count):
        return remote(
            tiles.at[s, pl.ds(0, count)], tiles.at[s + 1, pl.ds(0, count)],
            tile_send.at[s], tile_recv.at[s + 1], following,
        )

    def tile_pair(s, count, first):
        return remote(
            tiles.at[s, pl.ds(0, count)], tiles.at[s, pl.ds(first, count)],
            tpair_send.at[s], tpair_recv.at[s], partner,
        )

    def give(s, first, count):
        return remote(
            given.at[s, pl.ds(first, count)], taken.at[s, pl.ds(first, count)],
            give_send.at[s], give_recv.at[s], partner,
        )

    row_id = lax.broadcasted_iota(jnp.int32, (rows, LANES), 0)
    lane_id = lax.broadcasted_iota(jnp.int32, (rows, LANES), 1)
    own_lane = (row_id // 8) * experts + me

    def columns_of(s, count):
        cols = []
        for b in range(count):
            tile = tiles[s, b]
            full = jnp.concatenate([tile] * groups, axis=0)
            cols.append(jnp.sum(jnp.where(lane_id == own_lane, full, 0.0), axis=1, keepdims=True))
        return jnp.concatenate(cols, axis=0)

    up_step = inner // 2
    down_step = width // 2

    def up_piece(s, count, i):
        x = blocks[s, 0:count * rows, :]
        cols = slice(i * up_step, (i + 1) * up_step)
        gate_pre = jnp.dot(x, w_gate[:, cols], preferred_element_type=jnp.float32)
        up_pre = jnp.dot(x, w_up[:, cols], preferred_element_type=jnp.float32)
        act = gate_pre * jax.nn.sigmoid(gate_pre) * up_pre
        hidden[0:count * rows, cols] = (act * columns_of(s, count)).astype(jnp.bfloat16)

    def down_piece(s, count, i, layout):
        cols = slice(i * down_step, (i + 1) * down_step)
        answer = jnp.dot(hidden[0:count * rows, :], w_down[:, cols], preferred_element_type=jnp.float32)
        for dst, dst_row, src_row, n in layout:
            dst[s, dst_row:dst_row + n, cols] = answer[src_row:src_row + n].astype(dst.dtype)

    middle = ((given, 0, 0, 2 * rows), (kept, 0, 2 * rows, 2 * rows))
    first = ((kept, 0, 0, rows), (given, 0, rows, rows))
    last = ((kept, rows, 0, rows), (given, rows, rows, rows))

    def pieces_of(s, count, layout):
        return [
            lambda: up_piece(s, count, 0),
            lambda: up_piece(s, count, 1),
            lambda: down_piece(s, count, 0, layout),
            lambda: down_piece(s, count, 1, layout),
        ]

    for q in range(ncuts):
        ring(0, 0, q).start()
        pair(0, 0, q, rows).start()
    tile_pair(0, 1, 1).start()
    for q in range(ncuts):
        pair(0, 0, q, rows).wait_recv()
        ring(0, 1, q).start()
    tile_pair(0, 1, 1).wait_recv()
    tile_ring(0, 2).start()
    for load in loads[:3]:
        load.wait()

    def arrivals(s, pieces):
        todo = list(pieces)
        for b in range(2):
            for q in range(ncuts):
                ring(s - 1, b, q).wait_recv()
                if isinstance(s, int) and s == half - 1:
                    if b == 0:
                        ring(s, b, q).start()
                else:
                    ring(s, b, q).start()
                pair(s, b, q, (2 + b) * rows).start()
                if b == 1 and q == ncuts - 1:
                    tile_ring(s - 1, 2).wait_recv()
                    tile_ring(s, 1 if isinstance(s, int) and s == half - 1 else 2).start()
                    tile_pair(s, 2, 2).start()
                left = 2 * ncuts - (b * ncuts + q)
                run = -(-len(todo) // left)
                for piece in todo[:run]:
                    piece()
                todo = todo[run:]

    def ready(s):
        for b in range(2):
            for q in range(ncuts):
                pair(s, b, q, (2 + b) * rows).wait_recv()
        tile_pair(s, 2, 2).wait_recv()

    arrivals(1, pieces_of(0, 2, first))
    give(0, 0, rows).start()

    def body(s, carry):
        ready(s - 1)
        arrivals(s, pieces_of(s - 1, 4, middle))
        give(s - 1, 0, 2 * rows).start()
        return carry

    lax.fori_loop(2, half - 1, body, 0)
    ready(half - 2)
    arrivals(half - 1, pieces_of(half - 2, 4, middle))
    give(half - 2, 0, 2 * rows).start()

    ready(half - 1)
    todo = pieces_of(half - 1, 4, middle)
    for q in range(ncuts):
        ring(half - 1, 0, q).wait_recv()
        pair(half, 0, q, rows).start()
        if q == ncuts - 1:
            tile_ring(half - 1, 1).wait_recv()
            tile_pair(half, 1, 1).start()
        todo[q]()
    for piece in todo[ncuts:]:
        piece()
    give(half - 1, 0, 2 * rows).start()
    for q in range(ncuts):
        pair(half, 0, q, rows).wait_recv()
    tile_pair(half, 1, 1).wait_recv()
    for piece in pieces_of(half, 2, last):
        piece()
    give(half, rows, rows).start()

    def send_sum(k, b, q):
        if isinstance(k, int) and k == 1:
            return remote(
                area(partial, k, b * rows, q), area(final, 1 - b, 0, q),
                sum_send.at[k, b, q], final_recv.at[1 - b, q], crossing if b == 0 else following,
            )
        return remote(
            area(partial, k, b * rows, q), area(partial, k - 1, b * rows, q),
            sum_send.at[k, b, q], sum_recv.at[k - 1, b, q], following,
        )

    def came(k, b, q):
        return remote(
            area(partial, k, b * rows, q), area(partial, k, b * rows, q),
            sum_send.at[k, b, q], sum_recv.at[k, b, q], following,
        )

    def add_up(k, b, incoming):
        for q in range(ncuts):
            r, c = cuts[q]
            at = (k, pl.ds(b * rows + r, cut_rows), pl.ds(c, cut_cols))
            total = kept[at] + taken[at].astype(jnp.float32)
            if incoming:
                came(k, b, q).wait_recv()
                total += partial[at].astype(jnp.float32)
            partial[at] = total.astype(jnp.bfloat16)
            send_sum(k, b, q).start()

    give(half - 1, 0, 2 * rows).wait_recv()
    add_up(half - 1, 0, False)
    give(half, rows, rows).wait_recv()
    add_up(half, 1, False)

    for load in loads[3:]:
        load.wait()
    x = blocks[0, 0:rows, :]
    gate_pre = jnp.dot(x, v_gate[...], preferred_element_type=jnp.float32)
    up_pre = jnp.dot(x, v_up[...], preferred_element_type=jnp.float32)
    act = (gate_pre * jax.nn.sigmoid(gate_pre) * up_pre).astype(jnp.bfloat16)
    shared[...] = jnp.dot(act, v_down[...], preferred_element_type=jnp.float32)

    def sums(j, carry):
        give(half - 1 - j, 0, 2 * rows).wait_recv()
        add_up(half - 1 - j, 0, True)
        add_up(half - j, 1, True)
        return carry

    lax.fori_loop(1, half - 2, sums, 0)
    give(1, 0, 2 * rows).wait_recv()
    add_up(1, 0, True)
    add_up(2, 1, True)
    add_up(1, 1, True)

    give(0, 0, rows).wait_recv()
    shared[...] += kept[0, 0:rows, :] + taken[0, 0:rows, :].astype(jnp.float32)
    for q in range(ncuts):
        r, c = cuts[q]
        for i in (1, 0):
            remote(
                area(final, i, 0, q), area(final, i, 0, q), sum_send.at[1, i, q], final_recv.at[i, q], following
            ).wait_recv()
        at = (pl.ds(r, cut_rows), pl.ds(c, cut_cols))
        total = shared[at]
        for i in range(2):
            total += final[(i,) + at].astype(jnp.float32)
        out_ref[at] = total.astype(jnp.bfloat16)

    def sent_blocks(s, carry):
        for b in range(2):
            for q in range(ncuts):
                ring(s, b, q).wait_send()
        tile_ring(s, 2).wait_send()
        return carry

    def sent_pairs(s, carry):
        for b in range(2):
            for q in range(ncuts):
                pair(s, b, q, (2 + b) * rows).wait_send()
        tile_pair(s, 2, 2).wait_send()
        give(s, 0, 2 * rows).wait_send()
        return carry

    def sent_sums(k, carry):
        for b in range(2):
            for q in range(ncuts):
                came(k, b, q).wait_send()
        return carry

    lax.fori_loop(0, half - 1, sent_blocks, 0)
    lax.fori_loop(1, half, sent_pairs, 0)
    lax.fori_loop(1, half, sent_sums, 0)
    for q in range(ncuts):
        ring(half - 1, 0, q).wait_send()
        pair(0, 0, q, rows).wait_send()
        pair(half, 0, q, rows).wait_send()
        came(half, 1, q).wait_send()
    tile_ring(half - 1, 1).wait_send()
    tile_pair(0, 1, 1).wait_send()
    tile_pair(half, 1, 1).wait_send()
    give(0, 0, rows).wait_send()
    give(half, rows, rows).wait_send()


def local(tokens, routes, gates, norm_gain, e_gate, e_up, e_down, s_gate, s_up, s_down):
    rows, width = tokens.shape
    inner = e_down.shape[1]
    half = lax.axis_size("ep") // 4
    steps = half + 1
    ncuts = ROW_CUTS * COL_CUTS
    bf16, f32 = jnp.bfloat16, jnp.float32
    dma = pltpu.SemaphoreType.DMA
    whole = pl.BlockSpec(memory_space=pltpu.VMEM)
    apart = pl.BlockSpec(memory_space=pl.ANY)
    return pl.pallas_call(
        functools.partial(layer_kernel, half),
        out_shape=jax.ShapeDtypeStruct((rows, width), bf16),
        in_specs=[whole] * 4 + [apart] * 6,
        out_specs=whole,
        scratch_shapes=[
            pltpu.VMEM((steps, 4 * rows, width), bf16),
            pltpu.VMEM((steps, 4, 8, LANES), f32),
            pltpu.VMEM((width, inner), bf16),
            pltpu.VMEM((width, inner), bf16),
            pltpu.VMEM((inner, width), bf16),
            pltpu.VMEM((width, inner), bf16),
            pltpu.VMEM((width, inner), bf16),
            pltpu.VMEM((inner, width), bf16),
            pltpu.VMEM((4 * rows, inner), bf16),
            pltpu.VMEM((steps, 2 * rows, width), f32),
            pltpu.VMEM((steps, 2 * rows, width), bf16),
            pltpu.VMEM((steps, 2 * rows, width), bf16),
            pltpu.VMEM((steps, 2 * rows, width), bf16),
            pltpu.VMEM((2, rows, width), bf16),
            pltpu.VMEM((rows, width), f32),
            dma((6,)),
            dma((steps, 2, ncuts)),
            dma((steps, 2, ncuts)),
            dma((steps, 2, ncuts)),
            dma((steps, 2, ncuts)),
            dma((steps,)),
            dma((steps,)),
            dma((steps,)),
            dma((steps,)),
            dma((steps,)),
            dma((steps,)),
            dma((steps, 2, ncuts)),
            dma((steps, 2, ncuts)),
            dma((2, ncuts)),
        ],
        compiler_params=pltpu.CompilerParams(
            collective_id=0, has_side_effects=True, vmem_limit_bytes=60 << 20
        ),
    )(tokens, routes, gates, norm_gain.reshape(1, width), e_gate, e_up, e_down, s_gate, s_up, s_down)


def solution(mesh):
    token_spec = P(("grp", "ep"), None)
    expert_spec = P("ep", None, None)
    return jax.shard_map(
        local,
        mesh=mesh,
        in_specs=(token_spec, token_spec, token_spec, P(), expert_spec, expert_spec, expert_spec, P(), P(), P()),
        out_specs=token_spec,
        check_vma=False,
    )
```

time: 236 us -> 79.7 us (0.34)
  waiting for transfers between devices: 90.7 us -> 0 us
  Pallas kernels: 0 us -> 75.2 us
  blocking collectives: 67.4 us -> 0 us
  other arithmetic: 30 us -> 0 us
  matrix products: 19.6 us -> 0 us
  between operations: 13.2 us -> 0.01 us
  local copies, waits for them, and re-layouts: 13.4 us -> 4.29 us
    reduce_scatter x2 -> x0, waiting for transfers between devices: 87.5 us -> none  [summed_rows(): x = lax.psum_scatter(x, axis, scatter_dimension=dim, tiled=True)]
    pallas_call x0 -> x1, Pallas kernels: none -> 75.2 us  [local(): pl.pallas_call(functools.partial(layer_kernel, half), out_shape=jax.Shape...]
    all_gather x2 -> x0, blocking collectives: 67.4 us -> none  [the longest x1 39.5 us: local(): lax.all_gather(gates.astype(jnp.bfloat16), EP, axis=0, tiled=True)]
    dot_general x4 -> x0, matrix products: 19.6 us -> none  [the longest x1 8.28 us: expert_rows(): jnp.dot(hidden, w_down, preferred_element_type=jnp.float32)]
    scatter-add x1 -> x0, other arithmetic: 18.8 us -> none  [local(): partial_value.at[source].add(weight[:, None] * answers.astype(jnp.float32))]
    gather x2 -> x0, local copies, waits for them, and re-layouts: 13 us -> none  [the longest x1 9.85 us: local(): jnp.take(gathered, source, axis=0)]
    convert_element_type x3 -> x0, other arithmetic: 7.68 us -> none  [the longest x1 6.01 us: local(): partial_value.astype(jnp.bfloat16)]
    unnamed x4 -> x3, local copies, waits for them, and re-layouts: 0.01 us -> 4.29 us
  transfers between devices with their start and end apart: 3 -> 0, of which waited for: 3 -> 0; matrix products, arithmetic and copies ran while one was open for 3% -> 0% of each run, Pallas kernels for 0% -> 0%
where the time goes in v1:
time: 79.7 us; the launch traced here: 79.5 us
  Pallas kernels  75.2 us (94%)
  local copies, waits for them, and re-layouts  4.29 us (5%)
    pallas_call x1, Pallas kernels, local(): pl.pallas_call(functools.partial(layer_kernel, half), out_shape=jax.Shape...  75.2 us
    unnamed x3, local copies, waits for them, and re-layouts  4.29 us

profile of v1, /device:TPU:70, one launch (start us, length us, event | category | flops | bytes accessed | tf_op | source)
XLA Modules:
  0.0 79.5 jit_solution(2888610796323875481)
XLA Ops:
  0.0 1.4 %copy.11.routes_ref = s32[32,8]{1,0:T(8,128)} copy(s32[32,8]{0,1:T(8,128)} %param.11) | data formatting | bytes 2048 | tf_op args[1]
  1.4 1.4 %copy.12.gates_ref = f32[32,8]{1,0:T(8,128)} copy(f32[32,8]{0,1:T(8,128)} %param.12) | data formatting | bytes 2048 | tf_op args[2]
  2.7 75.2 %shard_map.100 = bf16[32,2048]{1,0:T(8,128)(2,1)} custom-call(bf16[32,2048]{1,0:T(8,128)(2,1)} %tokens_ref.1, s32[32,8]{1,0:T(8,128)} %copy.11.routes_ref, f32[32,8]{1,0:T(8,128)} %copy.12.gates_ref, f32[1,2048]{1,0:T(1,128)} %bitcast.1, bf16[1,2048,512]{2,1,0:T(8,128)(2,1)} %e_gate.1, bf16[1,2048,512]{2,1,0:T(8,128)(2,1)} %e_up.1, ...), custom_call_target="tpu_custom_call" | custom-call | tf_op jit(solution)/shard_map/pallas_call | solution.py:372
  77.9 1.6 %copy.14 = bf16[32,2048]{1,0:T(8,128)(2,1)} copy(bf16[32,2048]{1,0:T(8,128)(2,1)} %shard_map.100) | data formatting | bytes 262144
